TPU v7x, 32 devices: a whole 2x2x4 slice. The times are simulated.
32 devices in a mesh: rep: 4 (over z), fs: 4 (over y, x), tp: 2 (over core).
Axes of the slice: x: 2, y: 2, z: 4, core: 2. Of those that a mesh axis runs over, the one named last changes fastest.
Arguments:
- inputs: bfloat16 [512, 2048], P(('rep', 'fs', 'tp')), may hold values from -6 to 6
- cotangent: bfloat16 [512, 2048], P(('rep', 'fs', 'tp')), may hold values from -6 to 6
- norm_gain: float32 [2048], replicated, may hold values from 0.1 to 1.9
- gate_weight: bfloat16 [2048, 2816], P(None, ('fs', 'tp')), may hold values from -0.125 to 0.125
- up_weight: bfloat16 [2048, 2816], P(None, ('fs', 'tp')), may hold values from -0.125 to 0.125
- down_weight: bfloat16 [2816, 2048], P(('fs', 'tp')), may hold values from -0.109375 to 0.109375
Outputs:
- input_grad: bfloat16 [512, 2048], P(('rep', 'fs', 'tp'))
- gain_grad: float32 [2048], replicated
- down_grad: float32 [2816, 2048], P(('fs', 'tp'), 'rep')
All inputs are finite; a program needn't handle non-finite values.
Results may differ from a plain program's by a relative error of at most 0.0066.
Values may be sent and summed in bfloat16 or wider, within the bound.
A program may use at most 64 MiB of HBM per device.

v0:
```python
import jax
import jax.numpy as jnp
from jax import lax
from jax.sharding import PartitionSpec as P

EPS = 1e-06


def across_tokens(left, right):
    return lax.dot_general(
        left, right, (((0,), (0,)), ((), ())), preferred_element_type=jnp.float32
    )


def across_columns(left, right):
    return lax.dot_general(
        left, right, (((1,), (1,)), ((), ())), preferred_element_type=jnp.float32
    )


def per_device(inputs, cotangent, norm_gain, gate_weight, up_weight, down_weight):
    whole_x, whole_dy = (
        lax.all_gather(inputs, ("fs", "tp"), axis=0, tiled=True),
        lax.all_gather(cotangent, ("fs", "tp"), axis=0, tiled=True),
    )
    xf = whole_x.astype(jnp.float32)
    inv = lax.rsqrt(jnp.mean(xf * xf, axis=-1, keepdims=True) + EPS)
    normed = xf * inv
    hidden_in = (normed * norm_gain).astype(jnp.bfloat16)
    gate = jnp.dot(hidden_in, gate_weight, preferred_element_type=jnp.float32)
    up = jnp.dot(hidden_in, up_weight, preferred_element_type=jnp.float32)
    sig = jax.nn.sigmoid(gate)
    act = gate * sig
    hidden = (act * up).astype(jnp.bfloat16)
    d_hidden = 0.5 * across_columns(whole_dy, down_weight)
    d_gate = (d_hidden * up * sig * (1.0 + gate * (1.0 - sig))).astype(jnp.bfloat16)
    d_up = (d_hidden * act).astype(jnp.bfloat16)
    own_rows = inputs.shape[0]
    d_in = lax.psum_scatter(
        across_columns(d_gate, gate_weight) + across_columns(d_up, up_weight),
        ("fs", "tp"),
        scatter_dimension=0,
        tiled=True,
    )
    offset = lax.axis_index(("fs", "tp")) * own_rows
    own_normed = lax.dynamic_slice_in_dim(normed, offset, own_rows, 0)
    own_inv = lax.dynamic_slice_in_dim(inv, offset, own_rows, 0)
    gain_grad = lax.psum(jnp.sum(d_in * own_normed, axis=0), ("rep", "fs", "tp"))
    scaled = d_in * norm_gain
    input_grad = (
        own_inv * (scaled - own_normed * jnp.mean(scaled * own_normed, axis=-1, keepdims=True))
    ).astype(jnp.bfloat16)
    input_grad, gain_grad = (input_grad, gain_grad)
    part_down = 0.5 * across_tokens(whole_dy, hidden)
    got_down = lax.all_to_all(
        part_down[None].astype(jnp.bfloat16), "rep", split_axis=1, concat_axis=0, tiled=True
    ).astype(jnp.float32)
    down_grad = jnp.sum(got_down, axis=0).T
    return (input_grad, gain_grad, down_grad)


def solution(mesh):
    return jax.shard_map(
        per_device,
        mesh=mesh,
        in_specs=(
            P(("rep", "fs", "tp"), None),
            P(("rep", "fs", "tp"), None),
            P(),
            P(None, ("fs", "tp")),
            P(None, ("fs", "tp")),
            P(("fs", "tp"), None),
        ),
        out_specs=(P(("rep", "fs", "tp"), None), P(), P(("fs", "tp"), "rep")),
        check_vma=False,
    )
```

profile of v0, /device:TPU:0, one launch (start us, length us, event | category | flops | bytes accessed | tf_op | source)
XLA Modules:
  0.0 166.7 jit_solution(2304956729085242355)
XLA Ops:
  7.2 0.0 copy-start
  7.2 0.0 reduce-scatter.2.cloned.1.call-start
  7.2 11.8 %all_gather.6 = bf16[128,2048]{1,0:T(8,128)(2,1)S(1)} all-gather(bf16[16,2048]{1,0:T(8,128)(2,1)} %param.6), channel_id=1, replica_groups=mesh['rep'=4,'fs'=4,'tp'=2] {'fs','tp'}, dimensions={0}, use_global_device_ids=true | all-gather | bytes 589824 | tf_op jit(solution)/shard_map/all_gather | solution.py:23
  19.0 0.2 fusion.2
  19.2 1.4 fusion.3
  20.6 0.0 copy-start.6
  20.7 0.0 copy-start.3
  20.7 0.6 fusion.4
  21.3 0.3 copy-done.6
  21.6 9.5 %all_gather.7 = bf16[128,2048]{1,0:T(8,128)(2,1)S(1)} all-gather(bf16[16,2048]{1,0:T(8,128)(2,1)S(1)} %copy-done.6), channel_id=1, replica_groups=mesh['rep'=4,'fs'=4,'tp'=2] {'fs','tp'}, dimensions={0}, use_global_device_ids=true | all-gather | bytes 589824 | tf_op jit(solution)/shard_map/all_gather | solution.py:24
  31.1 0.8 copy-done.1
  31.9 0.5 convolution_multiply_fusion.1
  32.4 0.5 fusion.6
  32.9 0.0 copy-done.2
  33.0 1.5 convolution_add_fusion
  34.5 0.0 reduce-scatter.2.cloned.1.call-update
  34.5 1.8 %fusion.1 = bf16[1,2048,352]{1,2,0:T(8,128)(2,1)S(1)} fusion(bf16[128,2048]{1,0:T(8,128)(2,1)} %copy-done.1, f32[128,352]{0,1:T(8,128)} %copy-done.5, f32[128,352]{0,1:T(8,128)} %copy-done.2), kind=kOutput, calls=%fused_computation.2 | convolution fusion | flops 186261504 | bytes 2326528 | tf_op jit(solution)/shard_map/dot_general | solution.py:10
  36.3 5.7 %copy.12 = bf16[1,2048,352]{2,0,1:T(2,128)(2,1)} copy(bf16[1,2048,352]{1,2,0:T(8,128)(2,1)S(1)} %fusion.1) | data formatting | bytes 2883584 | tf_op jit(solution)/shard_map/convert_element_type | solution.py:56
  42.0 0.5 broadcast.53
  42.5 34.4 %reduce = bf16[2048,352]{1,0:T(8,128)(2,1)S(1)} reduce(bf16[2048,1,352]{2,1,0:T(2,128)(2,1)} %bitcast.16, bf16[]{:T(256)} %broadcast.53), dimensions={1}, to_apply=%bitcast.7.reduce_sub_computation | reduce | bytes 2883586
  76.9 3.6 %reshape.41 = bf16[4,2,90112]{2,1,0:T(2,128)(2,1)} reshape(bf16[2048,352]{1,0:T(8,128)(2,1)S(1)} %reduce) | data formatting | bytes 2883584
  80.5 4.9 %all-to-all-start = ((bf16[4,2,90112]{2,1,0:T(2,128)(2,1)}), bf16[4,2,90112]{2,1,0:T(2,128)(2,1)S(1)}, u32[]{:S(2)}, u32[]{:S(2)}) async-start(bf16[4,2,90112]{2,1,0:T(2,128)(2,1)} %reshape.41), calls=%async_computation.1 | async-start | bytes 2883584 | tf_op jit(solution)/shard_map/all_to_all | solution.py:55
  85.3 0.1 dynamic-slice.3
  85.4 1.1 convert_multiply_fusion
  86.5 1.1 multiply_reduce_fusion
  87.6 51.7 %psum.7 = f32[2048]{0:T(1024)} all-reduce(f32[2048]{0:T(1024)S(1)} %get-tuple-element.3), channel_id=1, replica_groups=mesh['rep'=4,'fs'=4,'tp'=2] {'rep','fs','tp'}, use_global_device_ids=true, to_apply=%region_4.0 | all-reduce | flops 2048 | bytes 16384 | tf_op jit(solution)/shard_map/psum | solution.py:48
  139.4 1.7 %multiply_convert_fusion.6 = bf16[16,2048]{1,0:T(8,128)(2,1)} fusion(f32[16,2048]{1,0:T(8,128)} %reduce-scatter.2.cloned.1.call-done, f32[128,2048]{1,0:T(8,128)} %convert_multiply_fusion, s32[]{:T(128)S(6)} %select_n.4, f32[16]{0:T(128)S(1)} %broadcast_multiply_fusion, f32[2048]{0:T(1024)S(1)} %copy-done.7, f32[16]{0:T(128)S(1)} %dynamic-slice.3), kind=kLoop, calls=%fused_computation.17 | loop fusion | flops 163840 | bytes 336004 | tf_op jit(solution)/shard_map/convert_element_type | solution.py:52
  141.0 0.0 all-to-all-done
  141.1 4.0 %reshape.42 = bf16[2048,1,352]{2,1,0:T(2,128)(2,1)} reshape(bf16[4,2,90112]{2,1,0:T(2,128)(2,1)S(1)} %all-to-all-done) | data formatting | bytes 2883584
  145.0 7.0 %copy.13 = bf16[1,2048,352]{1,2,0:T(8,128)(2,1)S(1)} copy(bf16[1,2048,352]{2,0,1:T(2,128)(2,1)} %bitcast.17) | data formatting | bytes 2883584 | tf_op jit(solution)/shard_map/all_to_all | solution.py:55
  152.0 3.4 %reshape.40 = f32[4,512,352]{1,0,2:T(4,128)} reshape(bf16[1,2048,352]{1,2,0:T(8,128)(2,1)S(1)} %copy.13) | data formatting | bytes 4325376 | tf_op jit(solution)/shard_map/convert_element_type | solution.py:57
  155.5 4.4 %reduce_sum.39 = f32[512,352]{0,1:T(8,128)} reduce(f32[4,512,352]{1,0,2:T(4,128)} %reshape.40, f32[]{:T(128)} %constant.11.clone.1), dimensions={0}, to_apply=%region_5.0 | reduce | flops 540672 | bytes 3604484 | tf_op jit(solution)/shard_map/reduce_sum | solution.py:58
  (13 shorter events, 0.0 us)
Async XLA Ops:
  7.2 12.0 %copy-start = (bf16[2048,352]{0,1:T(8,128)(2,1)S(1)}, bf16[2048,352]{0,1:T(8,128)(2,1)}, u32[]{:S(2)}) copy-start(bf16[2048,352]{0,1:T(8,128)(2,1)} %param.9) | copy-start | bytes 4325380
  7.2 79.3 %reduce-scatter.2.cloned.1.call-start = ((), (), s32[]{:S(2)}) async-start(), calls=%async_computation.2 | async-start | bytes 1179648 | tf_op jit(solution)/shard_map/reduce_scatter | solution.py:39
  19.0 1.6 copy-start.4
  19.0 1.6 copy-start.7
  20.6 12.3 %copy-start.2 = (f32[128,352]{0,1:T(8,128)}, f32[128,352]{0,1:T(8,128)S(1)}, u32[]{:S(2)}) copy-start(f32[128,352]{0,1:T(8,128)S(1)} %fusion.3) | copy-start | bytes 540676
  20.6 0.9 copy-start.6
  20.7 11.2 %copy-start.3 = (bf16[352,2048]{1,0:T(8,128)(2,1)S(1)}, bf16[352,2048]{1,0:T(8,128)(2,1)}, u32[]{:S(2)}) copy-start(bf16[352,2048]{1,0:T(8,128)(2,1)} %param.11) | copy-start | bytes 4325380
  21.6 11.4 %copy-start.5 = (f32[128,352]{0,1:T(8,128)}, f32[128,352]{0,1:T(8,128)S(1)}, u32[]{:S(2)}) copy-start(f32[128,352]{0,1:T(8,128)S(1)} %fusion.4) | copy-start | bytes 540676
  31.1 0.8 copy-start.1
  80.5 60.6 %all-to-all-start = ((bf16[4,2,90112]{2,1,0:T(2,128)(2,1)}), bf16[4,2,90112]{2,1,0:T(2,128)(2,1)S(1)}, u32[]{:S(2)}, u32[]{:S(2)}) async-start(bf16[4,2,90112]{2,1,0:T(2,128)(2,1)} %reshape.41), calls=%async_computation.1 | async-start | bytes 2883584 | tf_op jit(solution)/shard_map/all_to_all | solution.py:55
Sparse Core Ops, SparseCore 0:
  34.6 36.2 reduce-scatter.1
where the time goes:
time: 167 us
  blocking collectives  73 us (44%)
  other arithmetic  42.9 us (26%)
  local copies, waits for them, and re-layouts  25.4 us (15%)
  between operations  14.2 us (9%)
  matrix products  6.35 us (4%)
  starting transfers between devices  4.91 us (3%)
    psum x1, blocking collectives, per_device(): lax.psum(jnp.sum(d_in * own_normed, axis=0), ('rep', 'fs', 'tp'))  51.7 us
    unnamed x1, other arithmetic  34.4 us
    all_gather x1, blocking collectives, per_device(): lax.all_gather(inputs, ('fs', 'tp'), axis=0, tiled=True)  11.8 us
    all_gather x1, blocking collectives, per_device(): lax.all_gather(cotangent, ('fs', 'tp'), axis=0, tiled=True)  9.52 us
    unnamed x19, local copies, waits for them, and re-layouts  9.19 us
    all_to_all x1, local copies, waits for them, and re-layouts, per_device(): lax.all_to_all(part_down[None].astype(jnp.bfloat16), 'rep', split_axis=1,...  7.01 us
    convert_element_type x1, local copies, waits for them, and re-layouts, per_device(): part_down[None].astype(jnp.bfloat16)  5.72 us
    all_to_all x1, starting transfers between devices, per_device(): lax.all_to_all(part_down[None].astype(jnp.bfloat16), 'rep', split_axis=1,...  4.87 us
  transfers between devices with their start and end apart: 2, of which 0 were waited for; matrix products, arithmetic and copies ran while one was open for 30% of the time, Pallas kernels for 0%

commit v1 on v0

--- a/solution.py
+++ b/solution.py
@@ -1,6 +1,10 @@
+import functools
+
 import jax
 import jax.numpy as jnp
 from jax import lax
+from jax.experimental import pallas as pl
+from jax.experimental.pallas import tpu as pltpu
 from jax.sharding import PartitionSpec as P
 
 EPS = 1e-06
@@ -59,9 +63,246 @@
     return (input_grad, gain_grad, down_grad)
 
 
+MESH = pl.DeviceIdType.MESH
+LANES = 128
+PIECES = 2
+
+
+def kernel(
+    nr, nf,
+    x_ref, dy_ref, gain_ref, wg_hbm, wu_hbm, wd_hbm,
+    dx_ref, dgain_ref, ddown_ref,
+    wg, wu, wd, xg, dyg, dyc, own_hid, hid, normed, d_in, d_out, d_got, gz_own, gz, gg_own, gg,
+    w_sem, x_s, x_r, xs_s, xs_r, y_s, y_r, ys_s, ys_r, cz_s, cz_r, c_s, c_r, cs_s, cs_r,
+    h_s, h_r, d_s, d_r, gz_s, gz_r, gg_s, gg_r,
+):
+    r, f, t = lax.axis_index("rep"), lax.axis_index("fs"), lax.axis_index("tp")
+    ng = 2 * nf
+    me = 2 * f + t
+    own, width = x_ref.shape
+    cols = ddown_ref.shape[1]
+    sibling = (r, f, 1 - t)
+
+    def chip(k):
+        return lax.rem(f + k + nf, nf)
+
+    def layer(k):
+        return lax.rem(r + k + nr, nr)
+
+    def member(k):
+        g = lax.rem(me + k + ng, ng)
+        return g, (r, g // 2, lax.rem(g, 2))
+
+    def rows(g):
+        return pl.ds(pl.multiple_of(g * own, own), own)
+
+    def span(p):
+        return pl.ds(pl.multiple_of(p * cols, LANES), cols)
+
+    sent = []
+
+    def send(src, dst, ssem, rsem, to):
+        copy = pltpu.make_async_remote_copy(
+            src_ref=src, dst_ref=dst, send_sem=ssem, recv_sem=rsem,
+            device_id=to, device_id_type=MESH,
+        )
+        copy.start()
+        sent.append(copy)
+
+    def arrived(dst, ssem, rsem):
+        pltpu.make_async_remote_copy(
+            src_ref=dst, dst_ref=dst, send_sem=ssem, recv_sem=rsem,
+            device_id=sibling, device_id_type=MESH,
+        ).wait_recv()
+
+    loads = [
+        pltpu.make_async_copy(src, dst, w_sem.at[i])
+        for i, (src, dst) in enumerate(((wg_hbm, wg), (wu_hbm, wu), (wd_hbm, wd)))
+    ]
+    for load in loads:
+        load.start()
+
+    barrier = pltpu.get_barrier_semaphore()
+    for k in range(1, ng):
+        pl.semaphore_signal(barrier, inc=1, device_id=member(k)[1], device_id_type=MESH)
+    for k in range(1, nr):
+        pl.semaphore_signal(barrier, inc=1, device_id=(layer(k), f, t), device_id_type=MESH)
+    pl.semaphore_wait(barrier, ng - 1 + nr - 1)
+
+    for src, dst, ss, rs, bs, br in (
+        (x_ref, xg, x_s, x_r, xs_s, xs_r), (dy_ref, dyg, y_s, y_r, ys_s, ys_r)
+    ):
+        for k in range(1, nf):
+            send(src, dst.at[rows(me)], ss.at[k - 1], rs.at[k - 1], (r, chip(k), t))
+        send(src, dst.at[rows(me)], bs.at[0], br.at[0], sibling)
+    for k in range(1, nr):
+        to = layer(k)
+        send(
+            dy_ref.at[:, span(to)], dyc.at[k - 1, rows(me)],
+            cz_s.at[k - 1], cz_r.at[k - 1], (to, f, t),
+        )
+    xg[rows(me), :] = x_ref[...]
+    dyg[rows(me), :] = dy_ref[...]
+
+    def hand_on(ref, at, ss, rs, bs, br):
+        for k in range(1, nf):
+            block = at(ref, 2 * chip(-k) + t)
+            arrived(block, ss.at[k - 1], rs.at[k - 1])
+            send(block, block, bs.at[k], br.at[k], sibling)
+
+    def from_sibling(ref, at, bs, br):
+        for k in range(nf):
+            arrived(at(ref, 2 * chip(-k) + 1 - t), bs.at[k], br.at[k])
+
+    def plain(ref, g):
+        return ref.at[rows(g)]
+
+    def stacked(ref, g):
+        return ref.at[:, rows(g)]
+
+    hand_on(xg, plain, x_s, x_r, xs_s, xs_r)
+    from_sibling(xg, plain, xs_s, xs_r)
+
+    xf = xg[...].astype(jnp.float32)
+    inv = lax.rsqrt(jnp.mean(xf * xf, axis=-1, keepdims=True) + EPS)
+    normed[...] = xf * inv
+    hidden_in = (normed[...] * gain_ref[...]).astype(jnp.bfloat16)
+    for load in loads:
+        load.wait()
+    gate = jnp.dot(hidden_in, wg[...], preferred_element_type=jnp.float32)
+    up = jnp.dot(hidden_in, wu[...], preferred_element_type=jnp.float32)
+
+    hand_on(dyg, plain, y_s, y_r, ys_s, ys_r)
+    for k in range(1, nr):
+        arrived(dyc.at[k - 1, rows(me)], cz_s.at[k - 1], cz_r.at[k - 1])
+    for k in range(1, nf):
+        send(stacked(dyc, me), stacked(dyc, me), c_s.at[k - 1], c_r.at[k - 1], (r, chip(k), t))
+    send(stacked(dyc, me), stacked(dyc, me), cs_s.at[0], cs_r.at[0], sibling)
+    sig = jax.nn.sigmoid(gate)
+    act = gate * sig
+    own_hid[...] = (act * up).astype(jnp.bfloat16)
+    for k in range(1, nr):
+        send(own_hid, hid.at[k - 1], h_s.at[k - 1], h_r.at[k - 1], (layer(k), f, t))
+
+    from_sibling(dyg, plain, ys_s, ys_r)
+    d_hidden = 0.5 * across_columns(dyg[...], wd[...])
+    d_gate = (d_hidden * up * sig * (1.0 + gate * (1.0 - sig))).astype(jnp.bfloat16)
+    d_up = (d_hidden * act).astype(jnp.bfloat16)
+
+    step = width // PIECES
+    for p in range(PIECES):
+        part = slice(p * step, (p + 1) * step)
+        d_in[:, part] = across_columns(d_gate, wg[part, :]) + across_columns(d_up, wu[part, :])
+        d_out[:, part] = d_in[:, part].astype(jnp.bfloat16)
+        gz_own[:, part] = jnp.sum(d_in[:, part] * normed[:, part], axis=0, keepdims=True)
+        for k in range(1, ng):
+            g, to = member(k)
+            send(
+                d_out.at[rows(g), part], d_got.at[k - 1, :, part],
+                d_s.at[p, k - 1], d_r.at[p, k - 1], to,
+            )
+    for k in range(1, nr):
+        send(gz_own, gz.at[r], gz_s.at[k - 1], gz_r.at[k - 1], (layer(k), f, t))
+    gz[r] = gz_own[...]
+
+    hand_on(dyc, stacked, c_s, c_r, cs_s, cs_r)
+    total = across_tokens(own_hid[...], dyg[:, span(r)])
+
+    for k in range(1, nr):
+        arrived(gz.at[layer(-k)], gz_s.at[k - 1], gz_r.at[k - 1])
+    gg_own[...] = jnp.sum(gz[...], axis=0)
+    for k in range(1, ng):
+        send(gg_own, gg.at[me], gg_s.at[k - 1], gg_r.at[k - 1], member(k)[1])
+    gg[me] = gg_own[...]
+
+    from_sibling(dyc, stacked, cs_s, cs_r)
+    for k in range(1, nr):
+        arrived(hid.at[k - 1], h_s.at[k - 1], h_r.at[k - 1])
+        total = total + across_tokens(hid[k - 1], dyc[k - 1])
+    ddown_ref[...] = 0.5 * total
+
+    mine = d_in[rows(me), :]
+    for k in range(1, ng):
+        for p in range(PIECES):
+            arrived(
+                d_got.at[k - 1, :, slice(p * step, (p + 1) * step)],
+                d_s.at[p, k - 1], d_r.at[p, k - 1],
+            )
+        mine = mine + d_got[k - 1].astype(jnp.float32)
+    xf = x_ref[...].astype(jnp.float32)
+    own_inv = lax.rsqrt(jnp.mean(xf * xf, axis=-1, keepdims=True) + EPS)
+    own_normed = xf * own_inv
+    scaled = mine * gain_ref[...]
+    dx_ref[...] = (
+        own_inv * (scaled - own_normed * jnp.mean(scaled * own_normed, axis=-1, keepdims=True))
+    ).astype(jnp.bfloat16)
+
+    for k in range(1, ng):
+        arrived(gg.at[member(-k)[0]], gg_s.at[k - 1], gg_r.at[k - 1])
+    dgain_ref[...] = jnp.sum(gg[...], axis=0)
+    for copy in sent:
+        copy.wait_send()
+
+
+def fused(nr, nf, inputs, cotangent, norm_gain, gate_weight, up_weight, down_weight):
+    own, width = inputs.shape
+    share = gate_weight.shape[1]
+    ng = 2 * nf
+    group, cols = ng * own, width // nr
+    bf16, f32 = jnp.bfloat16, jnp.float32
+    vmem = pl.BlockSpec(memory_space=pltpu.VMEM)
+    hbm = pl.BlockSpec(memory_space=pl.ANY)
+    dma = pltpu.SemaphoreType.DMA
+    pair = lambda *n: [dma(n), dma(n)]
+    dx, dgain, ddown = pl.pallas_call(
+        functools.partial(kernel, nr, nf),
+        out_shape=(
+            jax.ShapeDtypeStruct((own, width), bf16),
+            jax.ShapeDtypeStruct((1, width), f32),
+            jax.ShapeDtypeStruct((share, cols), f32),
+        ),
+        in_specs=[vmem] * 3 + [hbm] * 3,
+        out_specs=(vmem,) * 3,
+        scratch_shapes=[
+            pltpu.VMEM((width, share), bf16),
+            pltpu.VMEM((width, share), bf16),
+            pltpu.VMEM((share, width), bf16),
+            pltpu.VMEM((group, width), bf16),
+            pltpu.VMEM((group, width), bf16),
+            pltpu.VMEM((nr - 1, group, cols), bf16),
+            pltpu.VMEM((group, share), bf16),
+            pltpu.VMEM((nr - 1, group, share), bf16),
+            pltpu.VMEM((group, width), f32),
+            pltpu.VMEM((group, width), f32),
+            pltpu.VMEM((group, width), bf16),
+            pltpu.VMEM((ng - 1, own, width), bf16),
+            pltpu.VMEM((1, width), f32),
+            pltpu.VMEM((nr, 1, width), f32),
+            pltpu.VMEM((1, width), f32),
+            pltpu.VMEM((ng, 1, width), f32),
+            dma((3,)),
+        ]
+        + pair(nf - 1) + pair(nf) + pair(nf - 1) + pair(nf)
+        + pair(nr - 1) + pair(nf - 1) + pair(nf)
+        + pair(nr - 1) + pair(PIECES, ng - 1) + pair(nr - 1) + pair(ng - 1),
+        compiler_params=pltpu.CompilerParams(
+            collective_id=0, has_side_effects=True, vmem_limit_bytes=48 * 1024 * 1024
+        ),
+    )(inputs, cotangent, norm_gain[None], gate_weight, up_weight, down_weight)
+    return dx, dgain[0], ddown
+
+
 def solution(mesh):
+    nr, nf, nt = (mesh.shape[name] for name in ("rep", "fs", "tp"))
+
+    def body(inputs, *others):
+        block = inputs.shape[1] // nr
+        if nt == 2 and nr > 1 and nf > 1 and block % LANES == 0 and inputs.shape[0] % 16 == 0:
+            return fused(nr, nf, inputs, *others)
+        return per_device(inputs, *others)
+
     return jax.shard_map(
-        per_device,
+        body,
         mesh=mesh,
         in_specs=(
             P(("rep", "fs", "tp"), None),

time: 167 us -> 37.3 us (0.22)
  blocking collectives: 73 us -> 0 us
  other arithmetic: 42.9 us -> 0 us
  Pallas kernels: 0 us -> 29.2 us
  local copies, waits for them, and re-layouts: 25.4 us -> 7.21 us
  between operations: 14.2 us -> 0.71 us
  matrix products: 6.35 us -> 0 us
  starting transfers between devices: 4.91 us -> 0 us
    psum x1 -> x0, blocking collectives: 51.7 us -> none  [per_device(): lax.psum(jnp.sum(d_in * own_normed, axis=0), ('rep', 'fs', 'tp'))]
    unnamed x1 -> x0, other arithmetic: 34.4 us -> none
    pallas_call x0 -> x1, Pallas kernels: none -> 29.2 us  [fused(): pl.pallas_call(functools.partial(kernel, nr, nf), out_shape=(jax.ShapeDty...]
    all_gather x2 -> x0, blocking collectives: 21.3 us -> none  [the longest x1 11.8 us: per_device(): lax.all_gather(inputs, ('fs', 'tp'), axis=0, tiled=True)]
    convert_element_type x2 -> x0, local copies, waits for them, and re-layouts: 9.15 us -> none  [the longest x1 5.72 us: per_device(): part_down[None].astype(jnp.bfloat16)]
    all_to_all x1 -> x0, local copies, waits for them, and re-layouts: 7.01 us -> none  [per_device(): lax.all_to_all(part_down[None].astype(jnp.bfloat16), 'rep', split_axis=1,...]
    dot_general x6 -> x0, matrix products: 6.35 us -> none  [the longest x3 2.56 us: across_columns(): lax.dot_general(left, right, (((1,), (1,)), ((), ())), preferred_element_...]
    reduce_sum x3 -> x0, other arithmetic: 5.69 us -> none  [the longest x1 4.38 us: per_device(): down_grad = jnp.sum(got_down, axis=0).T]
  transfers between devices with their start and end apart: 2 -> 0, of which waited for: 0 -> 0; matrix products, arithmetic and copies ran while one was open for 30% -> 0% of each run, Pallas kernels for 0% -> 0%
where the time goes in v1:
time: 37.3 us; the launch traced here: 37.1 us
  Pallas kernels  29.2 us (78%)
  local copies, waits for them, and re-layouts  7.21 us (19%)
  between operations  0.71 us (2%)
    pallas_call x1, Pallas kernels, fused(): pl.pallas_call(functools.partial(kernel, nr, nf), out_shape=(jax.ShapeDty...  29.2 us
    unnamed x13, local copies, waits for them, and re-layouts  7.21 us

profile of v1, /device:TPU:0, one launch (start us, length us, event | category | flops | bytes accessed | tf_op | source)
XLA Modules:
  0.0 37.1 jit_solution(4030822784187451945)
XLA Ops:
  0.6 1.9 %copy.9.wg_hbm = bf16[2048,352]{1,0:T(8,128)(2,1)S(1)} copy(bf16[2048,352]{0,1:T(8,128)(2,1)} %param.9) | data formatting | bytes 2883584 | tf_op args[3]
  2.5 0.0 copy-start.1
  2.5 0.0 copy-start.2
  2.5 0.0 copy-start.3
  2.5 1.9 %copy.10.wu_hbm = bf16[2048,352]{1,0:T(8,128)(2,1)S(1)} copy(bf16[2048,352]{0,1:T(8,128)(2,1)} %param.10) | data formatting | bytes 2883584 | tf_op args[4]
  4.4 0.0 copy-done.1
  4.4 0.0 copy-done.2
  4.4 0.0 copy-done.3
  4.5 0.0 copy-start
  4.5 1.4 %copy-done = bf16[352,2048]{1,0:T(8,128)(2,1)S(1)} copy-done((bf16[352,2048]{1,0:T(8,128)(2,1)S(1)}, bf16[352,2048]{1,0:T(8,128)(2,1)}, u32[]{:S(2)}) %copy-start) | copy-done | bytes 1441816
  5.8 29.2 %shard_map.85 = (bf16[16,2048]{1,0:T(8,128)(2,1)S(1)}, f32[1,2048]{1,0:T(1,128)S(1)}, f32[352,512]{1,0:T(8,128)S(1)}) custom-call(bf16[16,2048]{1,0:T(8,128)(2,1)S(1)} %copy-done.1, bf16[16,2048]{1,0:T(8,128)(2,1)S(1)} %copy-done.2, f32[1,2048]{1,0:T(1,128)S(1)} %bitcast.2, bf16[2048,352]{1,0:T(8,128)(2,1)S(1)} %copy.9.wg_hbm, ...), custom_call_target="tpu_custom_call" | custom-call | tf_op jit(solution)/shard_map/pallas_call | solution.py:257
  35.0 0.6 %copy.14 = bf16[16,2048]{1,0:T(8,128)(2,1)} copy(bf16[16,2048]{1,0:T(8,128)(2,1)S(1)} %get-tuple-element.12) | data formatting | bytes 131072
  35.6 0.6 %copy.15 = f32[2048]{0:T(1024)} copy(f32[2048]{0:T(1024)S(1)} %bitcast.3) | data formatting | bytes 16384
  36.2 0.9 %copy.16 = f32[352,512]{1,0:T(8,128)} copy(f32[352,512]{1,0:T(8,128)S(1)} %get-tuple-element.14) | data formatting | bytes 1441792
Async XLA Ops:
  2.5 1.9 %copy-start.1 = (bf16[16,2048]{1,0:T(8,128)(2,1)S(1)}, bf16[16,2048]{1,0:T(8,128)(2,1)}, u32[]{:S(2)}) copy-start(bf16[16,2048]{1,0:T(8,128)(2,1)} %x_ref.1) | copy-start | bytes 196612
  2.5 1.9 %copy-start.2 = (bf16[16,2048]{1,0:T(8,128)(2,1)S(1)}, bf16[16,2048]{1,0:T(8,128)(2,1)}, u32[]{:S(2)}) copy-start(bf16[16,2048]{1,0:T(8,128)(2,1)} %dy_ref.1) | copy-start | bytes 196612
  2.5 1.9 %copy-start.3 = (f32[2048]{0:T(1024)S(1)}, f32[2048]{0:T(1024)}, u32[]{:S(2)}) copy-start(f32[2048]{0:T(1024)} %param.8) | copy-start | bytes 24580
  4.5 1.4 %copy-start = (bf16[352,2048]{1,0:T(8,128)(2,1)S(1)}, bf16[352,2048]{1,0:T(8,128)(2,1)}, u32[]{:S(2)}) copy-start(bf16[352,2048]{1,0:T(8,128)(2,1)} %wd_hbm.1) | copy-start | bytes 4325380

commit v2 on v1

--- a/solution.py
+++ b/solution.py
@@ -169,8 +169,8 @@
     hidden_in = (normed[...] * gain_ref[...]).astype(jnp.bfloat16)
     for load in loads:
         load.wait()
-    gate = jnp.dot(hidden_in, wg[...], preferred_element_type=jnp.float32)
-    up = jnp.dot(hidden_in, wu[...], preferred_element_type=jnp.float32)
+    gate = across_columns(hidden_in, wg[...])
+    up = across_columns(hidden_in, wu[...])
 
     hand_on(dyg, plain, y_s, y_r, ys_s, ys_r)
     for k in range(1, nr):
@@ -192,7 +192,9 @@
     step = width // PIECES
     for p in range(PIECES):
         part = slice(p * step, (p + 1) * step)
-        d_in[:, part] = across_columns(d_gate, wg[part, :]) + across_columns(d_up, wu[part, :])
+        d_in[:, part] = jnp.dot(
+            d_gate, wg[:, part], preferred_element_type=jnp.float32
+        ) + jnp.dot(d_up, wu[:, part], preferred_element_type=jnp.float32)
         d_out[:, part] = d_in[:, part].astype(jnp.bfloat16)
         gz_own[:, part] = jnp.sum(d_in[:, part] * normed[:, part], axis=0, keepdims=True)
         for k in range(1, ng):
@@ -264,8 +266,8 @@
         in_specs=[vmem] * 3 + [hbm] * 3,
         out_specs=(vmem,) * 3,
         scratch_shapes=[
-            pltpu.VMEM((width, share), bf16),
-            pltpu.VMEM((width, share), bf16),
+            pltpu.VMEM((share, width), bf16),
+            pltpu.VMEM((share, width), bf16),
             pltpu.VMEM((share, width), bf16),
             pltpu.VMEM((group, width), bf16),
             pltpu.VMEM((group, width), bf16),
@@ -286,9 +288,9 @@
         + pair(nr - 1) + pair(nf - 1) + pair(nf)
         + pair(nr - 1) + pair(PIECES, ng - 1) + pair(nr - 1) + pair(ng - 1),
         compiler_params=pltpu.CompilerParams(
-            collective_id=0, has_side_effects=True, vmem_limit_bytes=48 * 1024 * 1024
+            collective_id=0, has_side_effects=True
         ),
-    )(inputs, cotangent, norm_gain[None], gate_weight, up_weight, down_weight)
+    )(inputs, cotangent, norm_gain[None], gate_weight.T, up_weight.T, down_weight)
     return dx, dgain[0], ddown
 
 

time: 37.3 us -> 36.5 us (0.979)
  local copies, waits for them, and re-layouts: 7.21 us -> 4.78 us
  Pallas kernels: 29.2 us -> 30.8 us
    unnamed x13 -> x3, local copies, waits for them, and re-layouts: 7.21 us -> 4.78 us
    pallas_call x1, Pallas kernels: 29.2 us -> 30.8 us  [fused(): pl.pallas_call(functools.partial(kernel, nr, nf), out_shape=(jax.ShapeDty...]
where the time goes in v2:
time: 36.5 us; the launch traced here: 36.2 us
  Pallas kernels  30.8 us (84%)
  local copies, waits for them, and re-layouts  4.78 us (13%)
  between operations  0.64 us (2%)
    pallas_call x1, Pallas kernels, fused(): pl.pallas_call(functools.partial(kernel, nr, nf), out_shape=(jax.ShapeDty...  30.8 us
    unnamed x3, local copies, waits for them, and re-layouts  4.78 us

profile of v2, /device:TPU:0, one launch (start us, length us, event | category | flops | bytes accessed | tf_op | source)
XLA Modules:
  0.0 36.2 jit_solution(7292530150879102982)
XLA Ops:
  0.6 30.8 %shard_map.85 = (bf16[16,2048]{1,0:T(8,128)(2,1)}, f32[1,2048]{1,0:T(1,128)}, f32[352,512]{1,0:T(8,128)}) custom-call(bf16[16,2048]{1,0:T(8,128)(2,1)} %x_ref.1, bf16[16,2048]{1,0:T(8,128)(2,1)} %dy_ref.1, f32[1,2048]{1,0:T(1,128)} %bitcast.6, bf16[352,2048]{1,0:T(8,128)(2,1)} %bitcast.4, bf16[352,2048]{1,0:T(8,128)(2,1)} %bitcast.5, bf16[352,2048]{1,0:T(8,128)(2,1)} %wd_hbm.1), custom_call_target="tpu_custom_call" | custom-call | tf_op jit(solution)/shard_map/pallas_call | solution.py:259
  31.4 1.5 %copy.12 = bf16[16,2048]{1,0:T(8,128)(2,1)} copy(bf16[16,2048]{1,0:T(8,128)(2,1)} %get-tuple-element.12) | data formatting | bytes 131072
  32.9 1.3 %copy.13 = f32[2048]{0:T(1024)} copy(f32[2048]{0:T(1024)} %bitcast.7) | data formatting | bytes 16384
  34.2 2.0 %copy.14 = f32[352,512]{1,0:T(8,128)} copy(f32[352,512]{1,0:T(8,128)} %get-tuple-element.14) | data formatting | bytes 1441792

commit v3 on v2

--- a/solution.py
+++ b/solution.py
@@ -65,16 +65,16 @@
 
 MESH = pl.DeviceIdType.MESH
 LANES = 128
-PIECES = 2
+PIECES = 4
 
 
 def kernel(
     nr, nf,
     x_ref, dy_ref, gain_ref, wg_hbm, wu_hbm, wd_hbm,
     dx_ref, dgain_ref, ddown_ref,
-    wg, wu, wd, xg, dyg, dyc, own_hid, hid, normed, d_in, d_out, d_got, gz_own, gz, gg_own, gg,
+    wg, wu, wd, xg, dyg, dyc, own_hid, hid, normed, d_in, d_out, d_pair, d_send, d_got, gz_own, gz, gg_own, gg,
     w_sem, x_s, x_r, xs_s, xs_r, y_s, y_r, ys_s, ys_r, cz_s, cz_r, c_s, c_r, cs_s, cs_r,
-    h_s, h_r, d_s, d_r, gz_s, gz_r, gg_s, gg_r,
+    h_s, h_r, p_s, p_r, d_s, d_r, gz_s, gz_r, gg_s, gg_r,
 ):
     r, f, t = lax.axis_index("rep"), lax.axis_index("fs"), lax.axis_index("tp")
     ng = 2 * nf
@@ -172,18 +172,18 @@
     gate = across_columns(hidden_in, wg[...])
     up = across_columns(hidden_in, wu[...])
 
+    sig = jax.nn.sigmoid(gate)
+    act = gate * sig
+    own_hid[...] = (act * up).astype(jnp.bfloat16)
+    for k in range(1, nr):
+        send(own_hid, hid.at[k - 1], h_s.at[k - 1], h_r.at[k - 1], (layer(k), f, t))
+
     hand_on(dyg, plain, y_s, y_r, ys_s, ys_r)
     for k in range(1, nr):
         arrived(dyc.at[k - 1, rows(me)], cz_s.at[k - 1], cz_r.at[k - 1])
     for k in range(1, nf):
         send(stacked(dyc, me), stacked(dyc, me), c_s.at[k - 1], c_r.at[k - 1], (r, chip(k), t))
     send(stacked(dyc, me), stacked(dyc, me), cs_s.at[0], cs_r.at[0], sibling)
-    sig = jax.nn.sigmoid(gate)
-    act = gate * sig
-    own_hid[...] = (act * up).astype(jnp.bfloat16)
-    for k in range(1, nr):
-        send(own_hid, hid.at[k - 1], h_s.at[k - 1], h_r.at[k - 1], (layer(k), f, t))
-
     from_sibling(dyg, plain, ys_s, ys_r)
     d_hidden = 0.5 * across_columns(dyg[...], wd[...])
     d_gate = (d_hidden * up * sig * (1.0 + gate * (1.0 - sig))).astype(jnp.bfloat16)
@@ -195,36 +195,47 @@
         d_in[:, part] = jnp.dot(
             d_gate, wg[:, part], preferred_element_type=jnp.float32
         ) + jnp.dot(d_up, wu[:, part], preferred_element_type=jnp.float32)
-        d_out[:, part] = d_in[:, part].astype(jnp.bfloat16)
-        gz_own[:, part] = jnp.sum(d_in[:, part] * normed[:, part], axis=0, keepdims=True)
-        for k in range(1, ng):
-            g, to = member(k)
-            send(
-                d_out.at[rows(g), part], d_got.at[k - 1, :, part],
-                d_s.at[p, k - 1], d_r.at[p, k - 1], to,
-            )
-    for k in range(1, nr):
-        send(gz_own, gz.at[r], gz_s.at[k - 1], gz_r.at[k - 1], (layer(k), f, t))
-    gz[r] = gz_own[...]
-
-    hand_on(dyc, stacked, c_s, c_r, cs_s, cs_r)
-    total = across_tokens(own_hid[...], dyg[:, span(r)])
-
-    for k in range(1, nr):
-        arrived(gz.at[layer(-k)], gz_s.at[k - 1], gz_r.at[k - 1])
-    gg_own[...] = jnp.sum(gz[...], axis=0)
+        d_out[:, :, :, part] = (
+            d_in[:, part].astype(jnp.bfloat16).reshape(nf, 2, own, step)
+        )
+        gg_own[:, part] = jnp.sum(d_in[:, part] * normed[:, part], axis=0, keepdims=True)
+        send(
+            d_out.at[:, 1 - t, :, part], d_pair.at[:, :, part], p_s.at[p], p_r.at[p], sibling
+        )
     for k in range(1, ng):
         send(gg_own, gg.at[me], gg_s.at[k - 1], gg_r.at[k - 1], member(k)[1])
     gg[me] = gg_own[...]
 
+    for p in range(PIECES):
+        part = slice(p * step, (p + 1) * step)
+        arrived(d_pair.at[:, :, part], p_s.at[p], p_r.at[p])
+        for k in range(1, nf):
+            to = chip(k)
+            d_send[k - 1, :, part] = (
+                d_in[rows(2 * to + t), part] + d_pair[to, :, part].astype(jnp.float32)
+            ).astype(jnp.bfloat16)
+            send(
+                d_send.at[k - 1, :, part], d_got.at[k - 1, :, part],
+                d_s.at[p, k - 1], d_r.at[p, k - 1], (r, to, t),
+            )
+
+    hand_on(dyc, stacked, c_s, c_r, cs_s, cs_r)
+    for k in range(1, ng):
+        arrived(gg.at[member(-k)[0]], gg_s.at[k - 1], gg_r.at[k - 1])
+    gz_own[...] = jnp.sum(gg[...], axis=0)
+    for k in range(1, nr):
+        send(gz_own, gz.at[r], gz_s.at[k - 1], gz_r.at[k - 1], (layer(k), f, t))
+    gz[r] = gz_own[...]
+    total = across_tokens(own_hid[...], dyg[:, span(r)])
+
     from_sibling(dyc, stacked, cs_s, cs_r)
     for k in range(1, nr):
         arrived(hid.at[k - 1], h_s.at[k - 1], h_r.at[k - 1])
         total = total + across_tokens(hid[k - 1], dyc[k - 1])
     ddown_ref[...] = 0.5 * total
 
-    mine = d_in[rows(me), :]
-    for k in range(1, ng):
+    mine = d_in[rows(me), :] + d_pair[f].astype(jnp.float32)
+    for k in range(1, nf):
         for p in range(PIECES):
             arrived(
                 d_got.at[k - 1, :, slice(p * step, (p + 1) * step)],
@@ -239,11 +250,22 @@
         own_inv * (scaled - own_normed * jnp.mean(scaled * own_normed, axis=-1, keepdims=True))
     ).astype(jnp.bfloat16)
 
-    for k in range(1, ng):
-        arrived(gg.at[member(-k)[0]], gg_s.at[k - 1], gg_r.at[k - 1])
-    dgain_ref[...] = jnp.sum(gg[...], axis=0)
+    for k in range(1, nr):
+        arrived(gz.at[layer(-k)], gz_s.at[k - 1], gz_r.at[k - 1])
+    dgain_ref[...] = jnp.sum(gz[...], axis=0)
     for copy in sent:
         copy.wait_send()
+
+
+def put(a, b, c, a_out, b_out, c_out, sem):
+    copies = [
+        pltpu.make_async_copy(src, dst, sem.at[i])
+        for i, (src, dst) in enumerate(((a, a_out), (b, b_out), (c, c_out)))
+    ]
+    for copy in copies:
+        copy.start()
+    for copy in copies:
+        copy.wait()
 
 
 def fused(nr, nf, inputs, cotangent, norm_gain, gate_weight, up_weight, down_weight):
@@ -253,10 +275,10 @@
     group, cols = ng * own, width // nr
     bf16, f32 = jnp.bfloat16, jnp.float32
     vmem = pl.BlockSpec(memory_space=pltpu.VMEM)
-    hbm = pl.BlockSpec(memory_space=pl.ANY)
+    hbm = pl.BlockSpec(memory_space=pltpu.HBM)
     dma = pltpu.SemaphoreType.DMA
     pair = lambda *n: [dma(n), dma(n)]
-    dx, dgain, ddown = pl.pallas_call(
+    results = pl.pallas_call(
         functools.partial(kernel, nr, nf),
         out_shape=(
             jax.ShapeDtypeStruct((own, width), bf16),
@@ -276,8 +298,10 @@
             pltpu.VMEM((nr - 1, group, share), bf16),
             pltpu.VMEM((group, width), f32),
             pltpu.VMEM((group, width), f32),
-            pltpu.VMEM((group, width), bf16),
-            pltpu.VMEM((ng - 1, own, width), bf16),
+            pltpu.VMEM((nf, 2, own, width), bf16),
+            pltpu.VMEM((nf, own, width), bf16),
+            pltpu.VMEM((nf - 1, own, width), bf16),
+            pltpu.VMEM((nf - 1, own, width), bf16),
             pltpu.VMEM((1, width), f32),
             pltpu.VMEM((nr, 1, width), f32),
             pltpu.VMEM((1, width), f32),
@@ -286,11 +310,19 @@
         ]
         + pair(nf - 1) + pair(nf) + pair(nf - 1) + pair(nf)
         + pair(nr - 1) + pair(nf - 1) + pair(nf)
-        + pair(nr - 1) + pair(PIECES, ng - 1) + pair(nr - 1) + pair(ng - 1),
+        + pair(nr - 1) + pair(PIECES) + pair(PIECES, nf - 1) + pair(nr - 1) + pair(ng - 1),
         compiler_params=pltpu.CompilerParams(
-            collective_id=0, has_side_effects=True
+            collective_id=0, has_side_effects=True, vmem_limit_bytes=52 * 1024 * 1024
         ),
     )(inputs, cotangent, norm_gain[None], gate_weight.T, up_weight.T, down_weight)
+    dx, dgain, ddown = pl.pallas_call(
+        put,
+        out_shape=tuple(jax.ShapeDtypeStruct(a.shape, a.dtype) for a in results),
+        in_specs=[vmem] * 3,
+        out_specs=(hbm,) * 3,
+        scratch_shapes=[dma((3,))],
+        compiler_params=pltpu.CompilerParams(vmem_limit_bytes=52 * 1024 * 1024),
+    )(*results)
     return dx, dgain[0], ddown
 
 

time: 36.5 us -> 29 us (0.79)
  Pallas kernels: 30.8 us -> 25.7 us
  local copies, waits for them, and re-layouts: 4.78 us -> 2.37 us
    pallas_call x1, Pallas kernels: 30.8 us -> 24.8 us  [fused(): pl.pallas_call(functools.partial(kernel, nr, nf), out_shape=(jax.ShapeDty...]
    unnamed x3 -> x6, local copies, waits for them, and re-layouts: 4.78 us -> 2.37 us
    pallas_call x0 -> x1, Pallas kernels: none -> 0.91 us  [fused(): pl.pallas_call(put, out_shape=tuple((jax.ShapeDtypeStruct(a.shape, a.dtyp...]
where the time goes in v3:
time: 29 us; the launch traced here: 28.8 us
  Pallas kernels  25.7 us (89%)
  local copies, waits for them, and re-layouts  2.37 us (8%)
  between operations  0.65 us (2%)
    pallas_call x1, Pallas kernels, fused(): pl.pallas_call(functools.partial(kernel, nr, nf), out_shape=(jax.ShapeDty...  24.8 us
    unnamed x6, local copies, waits for them, and re-layouts  2.37 us
    pallas_call x1, Pallas kernels, fused(): pl.pallas_call(put, out_shape=tuple((jax.ShapeDtypeStruct(a.shape, a.dtyp...  0.91 us

profile of v3, /device:TPU:0, one launch (start us, length us, event | category | flops | bytes accessed | tf_op | source)
XLA Modules:
  0.0 28.8 jit_solution(16401864126007729421)
XLA Ops:
  0.6 0.0 copy-start
  0.6 0.8 %copy-done = bf16[16,2048]{1,0:T(8,128)(2,1)S(1)} copy-done((bf16[16,2048]{1,0:T(8,128)(2,1)S(1)}, bf16[16,2048]{1,0:T(8,128)(2,1)}, u32[]{:S(2)}) %copy-start) | copy-done | bytes 65560
  1.5 0.0 copy-start.1
  1.5 0.8 %copy-done.1 = bf16[16,2048]{1,0:T(8,128)(2,1)S(1)} copy-done((bf16[16,2048]{1,0:T(8,128)(2,1)S(1)}, bf16[16,2048]{1,0:T(8,128)(2,1)}, u32[]{:S(2)}) %copy-start.1) | copy-done | bytes 65560
  2.3 0.0 copy-start.2
  2.3 0.7 %copy-done.2 = f32[2048]{0:T(1024)S(1)} copy-done((f32[2048]{0:T(1024)S(1)}, f32[2048]{0:T(1024)}, u32[]{:S(2)}) %copy-start.2) | copy-done | bytes 8216
  3.0 24.8 %shard_map.85 = (bf16[16,2048]{1,0:T(8,128)(2,1)S(1)}, f32[1,2048]{1,0:T(1,128)S(1)}, f32[352,512]{1,0:T(8,128)S(1)}) custom-call(bf16[16,2048]{1,0:T(8,128)(2,1)S(1)} %copy-done, bf16[16,2048]{1,0:T(8,128)(2,1)S(1)} %copy-done.1, f32[1,2048]{1,0:T(1,128)S(1)} %bitcast.4, bf16[352,2048]{1,0:T(8,128)(2,1)} %bitcast.5, bf16[352,2048]{1,0:T(8,128)(2,1)} %bitcast.6, ...), custom_call_target="tpu_custom_call" | custom-call | tf_op jit(solution)/shard_map/pallas_call | solution.py:281
  27.8 0.9 %shard_map.86 = (bf16[16,2048]{1,0:T(8,128)(2,1)}, f32[1,2048]{1,0:T(1,128)}, f32[352,512]{1,0:T(8,128)}) custom-call(bf16[16,2048]{1,0:T(8,128)(2,1)S(1)} %get-tuple-element.9.a, f32[1,2048]{1,0:T(1,128)S(1)} %get-tuple-element.10.b, f32[352,512]{1,0:T(8,128)S(1)} %get-tuple-element.11.c), custom_call_target="tpu_custom_call" | custom-call | tf_op jit(solution)/shard_map/pallas_call | solution.py:318
Async XLA Ops:
  0.6 0.8 %copy-start = (bf16[16,2048]{1,0:T(8,128)(2,1)S(1)}, bf16[16,2048]{1,0:T(8,128)(2,1)}, u32[]{:S(2)}) copy-start(bf16[16,2048]{1,0:T(8,128)(2,1)} %x_ref.1) | copy-start | bytes 196612
  1.5 0.8 %copy-start.1 = (bf16[16,2048]{1,0:T(8,128)(2,1)S(1)}, bf16[16,2048]{1,0:T(8,128)(2,1)}, u32[]{:S(2)}) copy-start(bf16[16,2048]{1,0:T(8,128)(2,1)} %dy_ref.1) | copy-start | bytes 196612
  2.3 0.7 %copy-start.2 = (f32[2048]{0:T(1024)S(1)}, f32[2048]{0:T(1024)}, u32[]{:S(2)}) copy-start(f32[2048]{0:T(1024)} %param.8) | copy-start | bytes 24580

commit v4 on v3

--- a/solution.py
+++ b/solution.py
@@ -70,16 +70,16 @@
 
 def kernel(
     nr, nf,
-    x_ref, dy_ref, gain_ref, wg_hbm, wu_hbm, wd_hbm,
+    x_hbm, dy_hbm, gain_hbm, wg_hbm, wu_hbm, wd_hbm,
     dx_ref, dgain_ref, ddown_ref,
-    wg, wu, wd, xg, dyg, dyc, own_hid, hid, normed, d_in, d_out, d_pair, d_send, d_got, gz_own, gz, gg_own, gg,
+    x_ref, dy_ref, gain_ref, wg, wu, wd, xg, dyg, dyc, own_hid, hid, normed, d_in, d_out, d_pair, d_send, d_got, gz_own, gz, gg_own, gg,
     w_sem, x_s, x_r, xs_s, xs_r, y_s, y_r, ys_s, ys_r, cz_s, cz_r, c_s, c_r, cs_s, cs_r,
     h_s, h_r, p_s, p_r, d_s, d_r, gz_s, gz_r, gg_s, gg_r,
 ):
     r, f, t = lax.axis_index("rep"), lax.axis_index("fs"), lax.axis_index("tp")
     ng = 2 * nf
     me = 2 * f + t
-    own, width = x_ref.shape
+    own, width = x_hbm.shape
     cols = ddown_ref.shape[1]
     sibling = (r, f, 1 - t)
 
@@ -117,7 +117,12 @@
 
     loads = [
         pltpu.make_async_copy(src, dst, w_sem.at[i])
-        for i, (src, dst) in enumerate(((wg_hbm, wg), (wu_hbm, wu), (wd_hbm, wd)))
+        for i, (src, dst) in enumerate(
+            (
+                (x_hbm, x_ref), (dy_hbm, dy_ref), (gain_hbm, gain_ref),
+                (wg_hbm, wg), (wu_hbm, wu), (wd_hbm, wd),
+            )
+        )
     ]
     for load in loads:
         load.start()
@@ -128,6 +133,8 @@
     for k in range(1, nr):
         pl.semaphore_signal(barrier, inc=1, device_id=(layer(k), f, t), device_id_type=MESH)
     pl.semaphore_wait(barrier, ng - 1 + nr - 1)
+    for load in loads[:3]:
+        load.wait()
 
     for src, dst, ss, rs, bs, br in (
         (x_ref, xg, x_s, x_r, xs_s, xs_r), (dy_ref, dyg, y_s, y_r, ys_s, ys_r)
@@ -167,7 +174,7 @@
     inv = lax.rsqrt(jnp.mean(xf * xf, axis=-1, keepdims=True) + EPS)
     normed[...] = xf * inv
     hidden_in = (normed[...] * gain_ref[...]).astype(jnp.bfloat16)
-    for load in loads:
+    for load in loads[3:]:
         load.wait()
     gate = across_columns(hidden_in, wg[...])
     up = across_columns(hidden_in, wu[...])
@@ -285,9 +292,12 @@
             jax.ShapeDtypeStruct((1, width), f32),
             jax.ShapeDtypeStruct((share, cols), f32),
         ),
-        in_specs=[vmem] * 3 + [hbm] * 3,
+        in_specs=[hbm] * 6,
         out_specs=(vmem,) * 3,
         scratch_shapes=[
+            pltpu.VMEM((own, width), bf16),
+            pltpu.VMEM((own, width), bf16),
+            pltpu.VMEM((1, width), f32),
             pltpu.VMEM((share, width), bf16),
             pltpu.VMEM((share, width), bf16),
             pltpu.VMEM((share, width), bf16),
@@ -306,7 +316,7 @@
             pltpu.VMEM((nr, 1, width), f32),
             pltpu.VMEM((1, width), f32),
             pltpu.VMEM((ng, 1, width), f32),
-            dma((3,)),
+            dma((6,)),
         ]
         + pair(nf - 1) + pair(nf) + pair(nf - 1) + pair(nf)
         + pair(nr - 1) + pair(nf - 1) + pair(nf)
@@ -314,7 +324,12 @@
         compiler_params=pltpu.CompilerParams(
             collective_id=0, has_side_effects=True, vmem_limit_bytes=52 * 1024 * 1024
         ),
-    )(inputs, cotangent, norm_gain[None], gate_weight.T, up_weight.T, down_weight)
+    )(*[
+        pltpu.with_memory_space_constraint(a, pltpu.HBM)
+        for a in (
+            inputs, cotangent, norm_gain[None], gate_weight.T, up_weight.T, down_weight
+        )
+    ])
     dx, dgain, ddown = pl.pallas_call(
         put,
         out_shape=tuple(jax.ShapeDtypeStruct(a.shape, a.dtype) for a in results),

time: 29 us -> 26.7 us (0.921)
  local copies, waits for them, and re-layouts: 2.37 us -> 0 us
    unnamed x6 -> x0, local copies, waits for them, and re-layouts: 2.37 us -> none
where the time goes in v4:
time: 26.7 us; the launch traced here: 26.5 us
  Pallas kernels  25.9 us (97%)
  between operations  0.64 us (2%)
    pallas_call x1, Pallas kernels, fused(): pl.pallas_call(functools.partial(kernel, nr, nf), out_shape=(jax.ShapeDty...  25 us
    pallas_call x1, Pallas kernels, fused(): pl.pallas_call(put, out_shape=tuple((jax.ShapeDtypeStruct(a.shape, a.dtyp...  0.91 us

profile of v4, /device:TPU:0, one launch (start us, length us, event | category | flops | bytes accessed | tf_op | source)
XLA Modules:
  0.0 26.5 jit_solution(9919985528432722905)
XLA Ops:
  0.6 25.0 %shard_map.85 = (bf16[16,2048]{1,0:T(8,128)(2,1)S(1)}, f32[1,2048]{1,0:T(1,128)S(1)}, f32[352,512]{1,0:T(8,128)S(1)}) custom-call(bf16[16,2048]{1,0:T(8,128)(2,1)} %x_hbm.1, bf16[16,2048]{1,0:T(8,128)(2,1)} %dy_hbm.1, f32[1,2048]{1,0:T(1,128)} %bitcast.6, bf16[352,2048]{1,0:T(8,128)(2,1)} %bitcast.4, bf16[352,2048]{1,0:T(8,128)(2,1)} %bitcast.5, ...), custom_call_target="tpu_custom_call" | custom-call | tf_op jit(solution)/shard_map/pallas_call | solution.py:288
  25.6 0.9 %shard_map.86 = (bf16[16,2048]{1,0:T(8,128)(2,1)}, f32[1,2048]{1,0:T(1,128)}, f32[352,512]{1,0:T(8,128)}) custom-call(bf16[16,2048]{1,0:T(8,128)(2,1)S(1)} %get-tuple-element.9.a, f32[1,2048]{1,0:T(1,128)S(1)} %get-tuple-element.10.b, f32[352,512]{1,0:T(8,128)S(1)} %get-tuple-element.11.c), custom_call_target="tpu_custom_call" | custom-call | tf_op jit(solution)/shard_map/pallas_call | solution.py:333

commit v5 on v4

--- a/solution.py
+++ b/solution.py
@@ -84,7 +84,14 @@
     sibling = (r, f, 1 - t)
 
     def chip(k):
-        return lax.rem(f + k + nf, nf)
+        if nf & (nf - 1):
+            return lax.rem(f + k + nf, nf)
+        partner, bit = f, 1
+        while bit < nf:
+            if abs(k) & bit:
+                partner = partner + bit - 2 * bit * lax.rem(partner // bit, 2)
+            bit *= 2
+        return partner
 
     def layer(k):
         return lax.rem(r + k + nr, nr)
@@ -234,12 +241,6 @@
         send(gz_own, gz.at[r], gz_s.at[k - 1], gz_r.at[k - 1], (layer(k), f, t))
     gz[r] = gz_own[...]
     total = across_tokens(own_hid[...], dyg[:, span(r)])
-
-    from_sibling(dyc, stacked, cs_s, cs_r)
-    for k in range(1, nr):
-        arrived(hid.at[k - 1], h_s.at[k - 1], h_r.at[k - 1])
-        total = total + across_tokens(hid[k - 1], dyc[k - 1])
-    ddown_ref[...] = 0.5 * total
 
     mine = d_in[rows(me), :] + d_pair[f].astype(jnp.float32)
     for k in range(1, nf):
@@ -256,6 +257,12 @@
     dx_ref[...] = (
         own_inv * (scaled - own_normed * jnp.mean(scaled * own_normed, axis=-1, keepdims=True))
     ).astype(jnp.bfloat16)
+
+    from_sibling(dyc, stacked, cs_s, cs_r)
+    for k in range(1, nr):
+        arrived(hid.at[k - 1], h_s.at[k - 1], h_r.at[k - 1])
+        total = total + across_tokens(hid[k - 1], dyc[k - 1])
+    ddown_ref[...] = 0.5 * total
 
     for k in range(1, nr):
         arrived(gz.at[layer(-k)], gz_s.at[k - 1], gz_r.at[k - 1])

time: 26.7 us -> 27.1 us (1.015)
  Pallas kernels: 25.9 us -> 26.3 us
    pallas_call x1, Pallas kernels: 25 us -> 25.4 us  [fused(): pl.pallas_call(functools.partial(kernel, nr, nf), out_shape=(jax.ShapeDty...]
where the time goes in v5:
time: 27.1 us; the launch traced here: 27 us
  Pallas kernels  26.3 us (97%)
  between operations  0.64 us (2%)
    pallas_call x1, Pallas kernels, fused(): pl.pallas_call(functools.partial(kernel, nr, nf), out_shape=(jax.ShapeDty...  25.4 us
    pallas_call x1, Pallas kernels, fused(): pl.pallas_call(put, out_shape=tuple((jax.ShapeDtypeStruct(a.shape, a.dtyp...  0.91 us

profile of v5, /device:TPU:0, one launch (start us, length us, event | category | flops | bytes accessed | tf_op | source)
XLA Modules:
  0.0 27.0 jit_solution(5182760117516144555)
XLA Ops:
  0.6 25.4 %shard_map.85 = (bf16[16,2048]{1,0:T(8,128)(2,1)S(1)}, f32[1,2048]{1,0:T(1,128)S(1)}, f32[352,512]{1,0:T(8,128)S(1)}) custom-call(bf16[16,2048]{1,0:T(8,128)(2,1)} %x_hbm.1, bf16[16,2048]{1,0:T(8,128)(2,1)} %dy_hbm.1, f32[1,2048]{1,0:T(1,128)} %bitcast.6, bf16[352,2048]{1,0:T(8,128)(2,1)} %bitcast.4, bf16[352,2048]{1,0:T(8,128)(2,1)} %bitcast.5, ...), custom_call_target="tpu_custom_call" | custom-call | tf_op jit(solution)/shard_map/pallas_call | solution.py:295
  26.1 0.9 %shard_map.86 = (bf16[16,2048]{1,0:T(8,128)(2,1)}, f32[1,2048]{1,0:T(1,128)}, f32[352,512]{1,0:T(8,128)}) custom-call(bf16[16,2048]{1,0:T(8,128)(2,1)S(1)} %get-tuple-element.9.a, f32[1,2048]{1,0:T(1,128)S(1)} %get-tuple-element.10.b, f32[352,512]{1,0:T(8,128)S(1)} %get-tuple-element.11.c), custom_call_target="tpu_custom_call" | custom-call | tf_op jit(solution)/shard_map/pallas_call | solution.py:340
